TPU v7x, 32 devices: a whole 2x2x4 slice. The times are simulated.
32 devices in a mesh: grp: 2 (over y), sp: 4 (over z), tp: 4 (over x, core).
Axes of the slice: x: 2, y: 2, z: 4, core: 2. Of those that a mesh axis runs over, the one named last changes fastest.
Arguments:
- tokens: bfloat16 [8, 512, 4096], P('grp', 'sp'), parts along dimension 0, may hold values from -9 to 9
- w_forget: bfloat16 [4096, 4096], P('sp', 'tp'), may hold values from -0.09375 to 0.09375
- w_value: bfloat16 [4096, 4096], P('sp', 'tp'), may hold values from -0.09375 to 0.09375
- lower_bound: float32 [4096], P('tp'), may hold values from 0.25 to 1
- decay_shift: float32 [8, 512, 32], P('grp', 'sp', 'tp'), parts along dimension 0, may hold values from -1 to 0
- queries: bfloat16 [8, 4096], P('grp', 'tp'), parts along dimension 0, may hold values from -6 to 6
- read_gain: float32 [4096], P('tp'), may hold values from 0.1 to 1.9
Outputs:
- cache_out: bfloat16 [8, 32, 16384], P('grp', 'tp', 'sp'), parts along dimension 0
- first_read: bfloat16 [8, 4096], P('grp', 'tp'), parts along dimension 0
There are 2 independent parts, one for each index of `grp`. A program takes and returns all parts, laid end to end along the dimension named above; an argument that names none is the same for every part. Nothing has to cross between parts.
All inputs are finite; a program needn't handle non-finite values.
Results may differ from a plain program's by a relative error of at most 0.01.
Values may be sent and summed in bfloat16 or wider, within the bound.
A program may use at most 128 MiB of HBM per device.

v0:
```python
import jax
import jax.numpy as jnp
from jax import lax
from jax.sharding import PartitionSpec as P

DK = 128
DV = 128


def entering(part, axis, combine, identity):
    count = lax.axis_size(axis)
    place = lax.axis_index(axis)
    ahead = count - 1 - place
    gathered = lax.all_gather(part, axis)
    state = jnp.zeros_like(part) + jnp.asarray(identity, part.dtype)

    def one(turn, state):
        source = count - 1 - turn
        return combine(state, lax.dynamic_index_in_dim(gathered, source, 0, False))

    return lax.fori_loop(0, ahead, one, state)


def add_terms(earlier, later_part):
    return earlier + later_part


def shards(tokens, w_forget, w_value, lower_bound, decay_shift, queries, read_gain):
    seq_count, span_len, feat_width = tokens.shape
    tok_rows = tokens.reshape(seq_count * span_len, feat_width)
    head_local = lower_bound.shape[0] // DK
    sp_count = lax.axis_size("sp")
    own_rows = DK // sp_count
    pre_gate = jnp.dot(
        tok_rows,
        lax.all_gather(w_forget, "sp", axis=0, tiled=True),
        preferred_element_type=jnp.float32,
    )
    value_sum = jnp.dot(
        tok_rows,
        lax.all_gather(w_value, "sp", axis=0, tiled=True),
        preferred_element_type=jnp.float32,
    )
    values = value_sum.astype(jnp.bfloat16)
    low_bound = lower_bound[None, :]
    log_forget = jnp.logaddexp(
        jnp.log(low_bound), jnp.log1p(-low_bound) + jax.nn.log_sigmoid(pre_gate)
    )
    log_forget = log_forget.reshape(seq_count, span_len, head_local, DK) + decay_shift[..., None]
    key_gates = ((1.0 - low_bound) * jax.nn.sigmoid(-pre_gate)).reshape(
        seq_count, span_len, head_local, DK
    )
    inclusive = jnp.cumsum(log_forget, axis=1)
    totals = inclusive[:, -1]
    weighted = (key_gates * jnp.exp(totals[:, None] - inclusive)).astype(jnp.bfloat16)
    span_values = values.reshape(seq_count, span_len, head_local, DV)
    local_state = jnp.einsum(
        "sthk,sthv->shkv", weighted, span_values, preferred_element_type=jnp.float32
    )
    suffix = entering(totals, "sp", add_terms, jnp.zeros_like(totals))
    decayed = (jnp.exp(suffix)[..., None] * local_state).reshape(seq_count, head_local, DK * DV)
    final_state = lax.psum_scatter(
        decayed.astype(jnp.bfloat16), "sp", scatter_dimension=2, tiled=True
    ).astype(jnp.float32)
    cache_out = final_state.astype(jnp.bfloat16)
    query_act = jax.nn.silu(queries.astype(jnp.float32)).reshape(seq_count, head_local, DK)
    own_query = lax.dynamic_slice_in_dim(query_act, lax.axis_index("sp") * own_rows, own_rows, 2)
    partial_value = jnp.sum(
        own_query[..., None] * final_state.reshape(seq_count, head_local, own_rows, DV), axis=2
    )
    total_read = lax.psum(partial_value, "sp")
    scaled = total_read * lax.rsqrt(
        jnp.mean(total_read * total_read, axis=-1, keepdims=True) + 1e-06
    )
    first_read = (
        (scaled * read_gain.reshape(head_local, DV))
        .reshape(seq_count, head_local * DV)
        .astype(jnp.bfloat16)
    )
    return (cache_out, first_read)


def solution(mesh):
    placed = (
        P("grp", "sp", None),
        P("sp", "tp"),
        P("sp", "tp"),
        P("tp"),
        P("grp", "sp", "tp"),
        P("grp", "tp"),
        P("tp"),
    )
    return jax.shard_map(
        shards,
        mesh=mesh,
        in_specs=placed,
        out_specs=(P("grp", "tp", "sp"), P("grp", "tp")),
        check_vma=False,
    )
```

profile of v0, /device:TPU:0, one launch (start us, length us, event | category | flops | bytes accessed | tf_op | source)
XLA Modules:
  0.0 376.4 jit_solution(16286272342859187152)
XLA Ops:
  7.2 0.7 all-gather.4.cloned.1.call-update
  8.0 0.7 all-gather.6.cloned.1.call-update
  8.7 0.1 copy.13
  8.9 153.0 %all-gather.4.cloned.1.call-done = bf16[4096,1024]{1,0:T(8,128)(2,1)} async-done(((bf16[1024,1024]{1,0:T(8,128)(2,1)}), bf16[4096,1024]{1,0:T(8,128)(2,1)}) %all-gather.4.cloned.1.call-update) | async-done | bytes 8388624 | tf_op jit(solution)/shard_map/all_gather | solution.py:36
  161.9 10.8 %select_bitcast_fusion = (f32[64,8,8,128]{3,1,2,0:T(8,128)S(1)}, f32[64,8,8,128]{3,1,2,0:T(8,128)S(1)}) fusion(f32[1024]{0:T(1024)S(1)} %get-tuple-element.73, f32[1024]{0:T(1024)S(1)} %get-tuple-element.71, f32[1024]{0:T(1024)S(1)} %get-tuple-element.72, bf16[512,4096]{1,0:T(8,128)(2,1)} %bitcast.55, bf16[4096,1024]{1,0:T(8,128)(2,1)} %all-gather.4.cloned.1.call-done), kind=kOutput, calls=%fused_computation.10 | convolution fusion | flops 4305453056 | bytes 16789504 | tf_op jit(solution)/shard_map/dot_general | solution.py:34
  172.7 0.5 copy.17
  173.2 1.8 copy.18
  175.0 0.8 fusion.3
  175.9 14.0 %all-gather = f32[16,1,8,128]{3,2,1,0:T(8,128)S(1)} all-gather(f32[4,1,8,128]{3,2,1,0:T(8,128)S(1)} %get-tuple-element.67), channel_id=2, replica_groups=mesh['grp'=2,'sp'=4,'tp'=4] {'sp'}, dimensions={0}, use_global_device_ids=true | all-gather | bytes 81920 | tf_op jit(solution)/shard_map/all_gather | solution.py:14
  189.8 0.1 while.12
  189.9 122.4 %all-gather.6.cloned.1.call-done = bf16[4096,1024]{1,0:T(8,128)(2,1)} async-done(((bf16[1024,1024]{1,0:T(8,128)(2,1)}), bf16[4096,1024]{1,0:T(8,128)(2,1)}) %all-gather.6.cloned.1.call-update) | async-done | bytes 8388624 | tf_op jit(solution)/shard_map/all_gather | solution.py:41
  312.3 9.1 %fusion.4 = bf16[64,8,8,128]{3,1,2,0:T(8,128)(2,1)S(1)} fusion(bf16[512,4096]{1,0:T(8,128)(2,1)} %bitcast.56, bf16[4096,1024]{1,0:T(8,128)(2,1)} %all-gather.6.cloned.1.call-done), kind=kOutput, calls=%fused_computation.12 | convolution fusion | flops 4295491584 | bytes 13631488 | tf_op jit(solution)/shard_map/dot_general | solution.py:39
  321.5 0.3 copy.19
  321.8 1.3 copy-done
  323.1 0.4 fusion.2
  323.5 1.1 multiply_convert_fusion
  324.7 1.3 convert_element_type.26
  326.0 0.1 constant_dynamic-slice_fusion
  326.1 0.1 copy.16
  326.2 25.4 %reduce-scatter.2.cloned.1.call-done = bf16[4,8,4096]{2,1,0:T(8,128)(2,1)} async-done(((bf16[4,8,16384]{2,1,0:T(8,128)(2,1)}), bf16[4,8,4096]{2,1,0:T(8,128)(2,1)}) %reduce-scatter.2.cloned.1.call-update) | async-done | bytes 262160 | tf_op jit(solution)/shard_map/reduce_scatter | solution.py:62
  351.6 1.2 fusion.8
  352.8 16.3 %psum.7 = f32[4,8,128]{2,1,0:T(8,128)S(1)} all-reduce(f32[4,8,128]{2,1,0:T(8,128)S(1)} %fusion.8), channel_id=1, replica_groups=mesh['grp'=2,'sp'=4,'tp'=4] {'sp'}, use_global_device_ids=true, to_apply=%region_5.6 | all-reduce | flops 4096 | bytes 32768 | tf_op jit(solution)/shard_map/psum | solution.py:71
  369.1 0.1 multiply_reduce_fusion
  369.2 0.6 copy.29
  (24 shorter events, 0.3 us)
Async XLA Ops:
  7.2 1.6 copy-start.1
  7.2 1.7 copy-start.4
  7.2 154.7 %all-gather.4.cloned.1.call-start = ((), (), s32[]{:S(2)}) async-start(), calls=%async_computation.1 | async-start | bytes 10485760 | tf_op jit(solution)/shard_map/all_gather | solution.py:36
  7.9 304.4 %all-gather.6.cloned.1.call-start = ((), (), s32[]{:S(2)}) async-start(), calls=%async_computation.2 | async-start | bytes 10485760 | tf_op jit(solution)/shard_map/all_gather | solution.py:41
  8.7 342.9 %reduce-scatter.2.cloned.1.call-start = ((), (), s32[]{:S(2)}) async-start(), calls=%async_computation.3 | async-start | bytes 1310720 | tf_op jit(solution)/shard_map/reduce_scatter | solution.py:62
  321.5 1.6 copy-start
  324.6 1.3 copy-start.2
  324.6 44.5 %copy-start.3 = (f32[1024]{0:T(1024)S(1)}, f32[1024]{0:T(1024)}, u32[]{:S(2)}) copy-start(f32[1024]{0:T(1024)} %param.15) | copy-start | bytes 12292
Sparse Core Ops, SparseCore 0:
  9.6 152.3 all-gather.3
  163.5 148.7 all-gather.5
  326.1 25.4 reduce-scatter.1
where the time goes:
time: 377 us; the launch traced here: 376 us
  waiting for transfers between devices  302 us (80%)
  blocking collectives  30.3 us (8%)
  matrix products  21 us (6%)
  between operations  13.9 us (4%)
  local copies, waits for them, and re-layouts  6.06 us (2%)
    all_gather x1, waiting for transfers between devices, shards(): lax.all_gather(w_forget, 'sp', axis=0, tiled=True)  153 us
    all_gather x1, waiting for transfers between devices, shards(): lax.all_gather(w_value, 'sp', axis=0, tiled=True)  122 us
    reduce_scatter x1, waiting for transfers between devices, shards(): lax.psum_scatter(decayed.astype(jnp.bfloat16), 'sp', scatter_dimension=2,...  25.4 us
    psum x1, blocking collectives, shards(): total_read = lax.psum(partial_value, 'sp')  16.3 us
    all_gather x1, blocking collectives, entering(): gathered = lax.all_gather(part, axis)  14 us
    dot_general x1, matrix products, shards(): jnp.dot(tok_rows, lax.all_gather(w_forget, 'sp', axis=0, tiled=True), pre...  10.8 us
    dot_general x1, matrix products, shards(): jnp.dot(tok_rows, lax.all_gather(w_value, 'sp', axis=0, tiled=True), pref...  9.14 us
  transfers between devices with their start and end apart: 3, of which 3 were waited for; matrix products, arithmetic and copies ran while one was open for 4% of the time, Pallas kernels for 0%

commit v1 on v0

--- a/solution.py
+++ b/solution.py
@@ -1,6 +1,10 @@
+import functools
+
 import jax
 import jax.numpy as jnp
 from jax import lax
+from jax.experimental import pallas as pl
+from jax.experimental.pallas import tpu as pltpu
 from jax.sharding import PartitionSpec as P
 
 DK = 128
@@ -80,6 +84,353 @@
     return (cache_out, first_read)
 
 
+SUB = 4
+
+
+def remote(src, dst, send_sem, recv_sem, **device):
+    return pltpu.make_async_remote_copy(
+        src_ref=src,
+        dst_ref=dst,
+        send_sem=send_sem,
+        recv_sem=recv_sem,
+        device_id=device,
+        device_id_type=pl.DeviceIdType.MESH,
+    )
+
+
+def kernel(
+    spans, tok_in, wf_in, wv_in, shift_in, low_ref, query_ref, gain_ref, cache_ref, read_ref,
+    tok, w_buf, shift, states, totals, out_send, out_recv, read_send, read_recv,
+    local_sem, z_send, z_recv, x_send, x_recv, d_send, d_recv,
+    w_send, w_recv, y_send, y_recv, s_send, s_recv, o_send, o_recv, r_send, r_recv,
+):
+    grp, z, tp = lax.axis_index("grp"), lax.axis_index("sp"), lax.axis_index("tp")
+    x_tp = tp + 2 - 4 * (tp // 2)
+    c_tp = tp + 1 - 2 * lax.rem(tp, 2)
+    xc_tp = x_tp + 1 - 2 * lax.rem(tp, 2)
+    seqs, span_len, _ = tok_in.shape
+    k_rows = wf_in.shape[0]
+    width = w_buf.shape[1] // 2
+    heads = width // DK
+    own_rows = DK // spans
+    sub_rows = span_len // SUB
+    steps = (spans - 1) * SUB
+
+    def rows_of(src):
+        return pl.ds(pl.multiple_of(src * k_rows, k_rows), k_rows)
+
+    def cols_of(j):
+        return pl.ds(pl.multiple_of(j * width, width), width)
+
+    locals_ = [
+        pltpu.make_async_copy(tok_in, tok.at[z], local_sem.at[0]),
+        pltpu.make_async_copy(wf_in.at[:, cols_of(z)], w_buf.at[rows_of(z), pl.ds(0, width)], local_sem.at[1]),
+        pltpu.make_async_copy(wv_in.at[:, cols_of(z)], w_buf.at[rows_of(z), pl.ds(width, width)], local_sem.at[2]),
+        pltpu.make_async_copy(shift_in, shift.at[z], local_sem.at[3]),
+    ]
+    for c in locals_:
+        c.start()
+
+    barrier = pltpu.get_barrier_semaphore()
+    for off in range(1, spans):
+        pl.semaphore_signal(barrier, inc=1, device_id={"sp": lax.rem(z + off, spans)}, device_id_type=pl.DeviceIdType.MESH)
+    pl.semaphore_signal(barrier, inc=1, device_id={"tp": x_tp}, device_id_type=pl.DeviceIdType.MESH)
+    pl.semaphore_signal(barrier, inc=1, device_id={"tp": c_tp}, device_id_type=pl.DeviceIdType.MESH)
+    pl.semaphore_signal(barrier, inc=1, device_id={"grp": 1 - grp}, device_id_type=pl.DeviceIdType.MESH)
+    pl.semaphore_wait(barrier, spans + 2)
+
+    def shift_copy(off):
+        return remote(shift_in, shift.at[z], s_send.at[off - 1], s_recv.at[z], sp=lax.rem(z + off, spans))
+
+    def weight_copy(w_in, off):
+        to = lax.rem(z + off, spans)
+        return remote(
+            w_in.at[:, cols_of(to)], w_buf.at[rows_of(z), cols_of(grp)], w_send.at[off - 1], w_recv.at[z], sp=to
+        )
+
+    def weight_pass(src):
+        part = w_buf.at[rows_of(src), cols_of(grp)]
+        return remote(part, part, y_send.at[src], y_recv.at[src], grp=1 - grp)
+
+    def piece(src, who, u):
+        return tok.at[src, who, pl.ds(pl.multiple_of(u * sub_rows, sub_rows), sub_rows)]
+
+    def z_copy(direction, src, u, to, from_input=False):
+        here = piece(src, tp, u)
+        start = tok_in.at[tp, pl.ds(pl.multiple_of(u * sub_rows, sub_rows), sub_rows)] if from_input else here
+        return remote(start, here, z_send.at[direction, src, u], z_recv.at[src, u], sp=to)
+
+    def x_copy(src, u):
+        here = piece(src, tp, u)
+        return remote(here, here, x_send.at[src, u], x_recv.at[src, u], tp=x_tp)
+
+    def d_copy(kind, src, u):
+        here = piece(src, tp if kind == 0 else x_tp, u)
+        return remote(here, here, d_send.at[kind, src, u], d_recv.at[kind, src, u], tp=c_tp)
+
+    for off in range(1, spans):
+        shift_copy(off).start()
+
+    @pl.when(grp == 0)
+    def _():
+        for off in range(1, spans):
+            weight_copy(wf_in, off).start()
+
+    @pl.when(grp == 1)
+    def _():
+        for off in range(1, spans):
+            weight_copy(wv_in, off).start()
+
+    signs = (1, -1)
+
+    def fits(place):
+        return jnp.logical_and(place >= 0, place < spans)
+
+    for direction, sign in enumerate(signs):
+        @pl.when(fits(z + sign))
+        def _():
+            def one(u, carry):
+                z_copy(direction, z, u, z + sign, True).start()
+                return carry
+
+            lax.fori_loop(0, SUB, one, 0)
+
+    for off in range(1, spans):
+        src = lax.rem(z + off, spans)
+        remote(wf_in.at[:, cols_of(0)], w_buf.at[rows_of(src), cols_of(grp)], w_send.at[off - 1], w_recv.at[src], sp=src).wait_recv()
+        weight_pass(src).start()
+    for off in range(1, spans):
+        src = lax.rem(z + off, spans)
+        remote(shift_in, shift.at[src], s_send.at[off - 1], s_recv.at[src], sp=src).wait_recv()
+    for c in locals_:
+        c.wait()
+
+    low = low_ref[:, cols_of(z)]
+    head_count = shift_in.shape[1]
+    pick = (
+        lax.broadcasted_iota(jnp.int32, (head_count, width), 0)
+        == z * heads + lax.broadcasted_iota(jnp.int32, (head_count, width), 1) // DK
+    ).astype(jnp.float32)
+    later_mask = (
+        lax.broadcasted_iota(jnp.int32, (span_len, span_len), 1)
+        > lax.broadcasted_iota(jnp.int32, (span_len, span_len), 0)
+    ).astype(jnp.float32)
+    exact = lax.Precision.HIGHEST
+
+    def compute(src, s):
+        both = jnp.dot(tok[src, s], w_buf[...], preferred_element_type=jnp.float32)
+        gates = (1.0 - low) * jax.nn.sigmoid(-both[:, :width])
+        decay = jnp.log1p(-gates) + lax.dot_general(
+            shift[src, s], pick, (((0,), (0,)), ((), ())), precision=exact, preferred_element_type=jnp.float32
+        )
+        later = jnp.dot(later_mask, decay, precision=exact, preferred_element_type=jnp.float32)
+        totals[src, s] = jnp.broadcast_to(jnp.sum(decay, axis=0, keepdims=True), (8, width))
+        weighted = (gates * jnp.exp(later)).astype(jnp.bfloat16)
+        vals = both[:, width:].astype(jnp.bfloat16)
+        for h in range(heads):
+            lanes = slice(h * DK, (h + 1) * DK)
+            states[src, s, h] = lax.dot_general(
+                vals[:, lanes], weighted[:, lanes], (((0,), (0,)), ((), ())), preferred_element_type=jnp.float32
+            )
+
+    def stage(n, carry):
+        far, u = n // SUB + 1, lax.rem(n, SUB)
+        for direction, sign in enumerate(signs):
+            src = z - far * sign
+
+            @pl.when(jnp.logical_and(n < steps, fits(src)))
+            def _():
+                z_copy(direction, src, u, z - sign).wait_recv()
+
+                @pl.when(fits(z + sign))
+                def _():
+                    z_copy(direction, src, u, z + sign).start()
+
+                x_copy(src, u).start()
+                d_copy(0, src, u).start()
+
+        last = jnp.maximum(n - 1, 0)
+        last_far, last_u = last // SUB + 1, lax.rem(last, SUB)
+        for direction, sign in enumerate(signs):
+            last_src = z - last_far * sign
+
+            @pl.when(jnp.logical_and(jnp.logical_and(n >= 1, n <= steps), fits(last_src)))
+            def _():
+                here = piece(last_src, x_tp, last_u)
+                remote(here, here, x_send.at[last_src, last_u], x_recv.at[last_src, last_u], tp=x_tp).wait_recv()
+                d_copy(1, last_src, last_u).start()
+
+        @pl.when(n == 1)
+        def _():
+            for off in range(1, spans):
+                src = lax.rem(z + off, spans)
+                part = w_buf.at[rows_of(src), cols_of(1 - grp)]
+                remote(part, part, y_send.at[src], y_recv.at[src], grp=1 - grp).wait_recv()
+
+        back = n - 1
+        done_far, slot = back // SUB, lax.rem(back, SUB)
+        who = jnp.where(slot == 0, tp, jnp.where(slot == 1, x_tp, jnp.where(slot == 2, c_tp, xc_tp)))
+
+        def one_side(direction, inner):
+            done_src = z - done_far * (1 - 2 * direction)
+            real = jnp.logical_and(fits(done_src), jnp.logical_or(done_far > 0, direction == 0))
+
+            @pl.when(jnp.logical_and(real, n >= 1))
+            def _():
+                for kind in range(2):
+                    @pl.when(jnp.logical_and(done_far > 0, slot == 2 + kind))
+                    def _():
+                        for v in range(SUB):
+                            here = piece(done_src, c_tp if kind == 0 else xc_tp, v)
+                            remote(here, here, d_send.at[kind, done_src, v], d_recv.at[kind, done_src, v], tp=c_tp).wait_recv()
+
+                compute(done_src, who)
+
+            return inner
+
+        return lax.fori_loop(0, 2, one_side, carry)
+
+    lax.fori_loop(0, spans * SUB + 1, stage, 0)
+
+    for s in range(seqs):
+        query = query_ref[pl.ds(s, 1), cols_of(z)]
+        query = query * jax.nn.sigmoid(query)
+        for h in range(heads):
+            lanes = slice(h * DK, (h + 1) * DK)
+            suffix = jnp.zeros((1, DK), jnp.float32)
+            turned = states[spans - 1, s, h]
+            for b in range(spans - 2, -1, -1):
+                suffix = suffix + totals[b + 1, s, 0:1, lanes]
+                turned = turned + jnp.exp(suffix) * states[b, s, h]
+            final = turned.T
+            for j in range(spans):
+                out_send[j, s, h] = final[j * own_rows:(j + 1) * own_rows].astype(jnp.bfloat16)
+            total = jnp.dot(query[:, lanes], final, precision=exact, preferred_element_type=jnp.float32)
+            scaled = total * lax.rsqrt(jnp.mean(total * total, axis=-1, keepdims=True) + 1e-06)
+            first = pl.multiple_of(z * width + h * DV, DV)
+            read_send[pl.ds(s, 1), lanes] = scaled * gain_ref[:, pl.ds(first, DV)]
+
+    def out_copy(off):
+        to = lax.rem(z + off, spans)
+        return remote(out_send.at[to], out_recv.at[z], o_send.at[off - 1], o_recv.at[z], sp=to)
+
+    def read_copy(off):
+        return remote(read_send, read_recv.at[z], r_send.at[off - 1], r_recv.at[z], sp=lax.rem(z + off, spans))
+
+    for off in range(1, spans):
+        out_copy(off).start()
+        read_copy(off).start()
+
+    for off in range(1, spans):
+        shift_copy(off).wait_send()
+        weight_copy(wf_in, off).wait_send()
+        weight_pass(lax.rem(z + off, spans)).wait_send()
+
+    def drain(n, carry):
+        far, u = n // SUB, lax.rem(n, SUB)
+        for direction, sign in enumerate(signs):
+            src = z - far * sign
+
+            @pl.when(jnp.logical_and(fits(src), fits(z + sign)))
+            def _():
+                z_copy(direction, src, u, z + sign).wait_send()
+
+            @pl.when(jnp.logical_and(fits(src), far > 0))
+            def _():
+                x_copy(src, u).wait_send()
+                d_copy(0, src, u).wait_send()
+                d_copy(1, src, u).wait_send()
+
+        return carry
+
+    lax.fori_loop(0, spans * SUB, drain, 0)
+
+    for off in range(1, spans):
+        src = lax.rem(z + off, spans)
+        remote(out_send.at[src], out_recv.at[src], o_send.at[off - 1], o_recv.at[src], sp=src).wait_recv()
+        remote(read_send, read_recv.at[src], r_send.at[off - 1], r_recv.at[src], sp=src).wait_recv()
+    for src in range(spans):
+        mine = z == src
+        cache_ref[:, src * heads:(src + 1) * heads] = jnp.where(mine, out_send[src], out_recv[src])
+        read_ref[:, src * width:(src + 1) * width] = jnp.where(mine, read_send[:seqs], read_recv[src, :seqs]).astype(jnp.bfloat16)
+    for off in range(1, spans):
+        out_copy(off).wait_send()
+        read_copy(off).wait_send()
+
+
+def fused(spans, tokens, w_forget, w_value, lower_bound, decay_shift, queries, read_gain):
+    seqs, span_len, feat = tokens.shape
+    k_rows, cols = w_forget.shape
+    width = cols // spans
+    heads = width // DK
+    own_rows = DK // spans
+    head_local = cols // DK
+    anywhere = pl.BlockSpec(memory_space=pl.ANY)
+    vmem = pl.BlockSpec(memory_space=pltpu.VMEM)
+    dma = pltpu.SemaphoreType.DMA
+    cache, read = pl.pallas_call(
+        functools.partial(kernel, spans),
+        out_shape=(
+            jax.ShapeDtypeStruct((seqs, head_local, own_rows, DV), jnp.bfloat16),
+            jax.ShapeDtypeStruct((seqs, cols), jnp.bfloat16),
+        ),
+        in_specs=[anywhere] * 3 + [vmem] * 4,
+        out_specs=(vmem, vmem),
+        scratch_shapes=[
+            pltpu.VMEM((spans, seqs, span_len, feat), jnp.bfloat16),
+            pltpu.VMEM((feat, 2 * width), jnp.bfloat16),
+            pltpu.VMEM((spans, seqs, head_local, span_len), jnp.float32),
+            pltpu.VMEM((spans, seqs, heads, DV, DK), jnp.float32),
+            pltpu.VMEM((spans, seqs, 8, width), jnp.float32),
+            pltpu.VMEM((spans, seqs, heads, own_rows, DV), jnp.bfloat16),
+            pltpu.VMEM((spans, seqs, heads, own_rows, DV), jnp.bfloat16),
+            pltpu.VMEM((8, width), jnp.float32),
+            pltpu.VMEM((spans, 8, width), jnp.float32),
+            dma((4,)),
+            dma((2, spans, SUB)),
+            dma((spans, SUB)),
+            dma((spans, SUB)),
+            dma((spans, SUB)),
+            dma((2, spans, SUB)),
+            dma((2, spans, SUB)),
+            dma((spans - 1,)),
+            dma((spans,)),
+            dma((spans,)),
+            dma((spans,)),
+            dma((spans - 1,)),
+            dma((spans,)),
+            dma((spans - 1,)),
+            dma((spans,)),
+            dma((spans - 1,)),
+            dma((spans,)),
+        ],
+        compiler_params=pltpu.CompilerParams(
+            collective_id=0, has_side_effects=True, vmem_limit_bytes=60 * 1024 * 1024
+        ),
+        name="gated_state",
+    )(
+        tokens,
+        w_forget,
+        w_value,
+        decay_shift.transpose(0, 2, 1),
+        lower_bound.reshape(1, -1),
+        queries.astype(jnp.float32),
+        read_gain.reshape(1, -1),
+    )
+    return cache.reshape(seqs, head_local, own_rows * DV), read
+
+
+def by_shape(tokens, w_forget, *rest):
+    spans, lanes, groups = (lax.axis_size(a) for a in ("sp", "tp", "grp"))
+    seqs, span_len, _ = tokens.shape
+    heads = w_forget.shape[1] // DK
+    fit = groups == 2 and lanes == 4 and seqs == lanes and heads % spans == 0
+    fit = fit and DK % (16 * spans) == 0 and heads % 8 == 0 and span_len == DK
+    if fit:
+        return fused(spans, tokens, w_forget, *rest)
+    return shards(tokens, w_forget, *rest)
+
+
 def solution(mesh):
     placed = (
         P("grp", "sp", None),
@@ -91,7 +442,7 @@
         P("tp"),
     )
     return jax.shard_map(
-        shards,
+        by_shape,
         mesh=mesh,
         in_specs=placed,
         out_specs=(P("grp", "tp", "sp"), P("grp", "tp")),

time: 377 us -> 160 us (0.42)
  waiting for transfers between devices: 302 us -> 0 us
  Pallas kernels: 0 us -> 154 us
  blocking collectives: 30.3 us -> 0 us
  matrix products: 21 us -> 0 us
  between operations: 13.9 us -> 0.64 us
    all_gather x2 -> x0, waiting for transfers between devices: 275 us -> none  [the longest x1 153 us: shards(): lax.all_gather(w_forget, 'sp', axis=0, tiled=True)]
    pallas_call x0 -> x1, Pallas kernels: none -> 154 us  [fused(): pl.pallas_call(functools.partial(kernel, spans), out_shape=(jax.ShapeDtyp...]
    reduce_scatter x1 -> x0, waiting for transfers between devices: 25.4 us -> none  [shards(): lax.psum_scatter(decayed.astype(jnp.bfloat16), 'sp', scatter_dimension=2,...]
    dot_general x3 -> x0, matrix products: 21 us -> none  [the longest x1 10.8 us: shards(): jnp.dot(tok_rows, lax.all_gather(w_forget, 'sp', axis=0, tiled=True), pre...]
    psum x1 -> x0, blocking collectives: 16.3 us -> none  [shards(): total_read = lax.psum(partial_value, 'sp')]
    all_gather x1 -> x0, blocking collectives: 14 us -> none  [entering(): gathered = lax.all_gather(part, axis)]
  transfers between devices with their start and end apart: 3 -> 0, of which waited for: 3 -> 0; matrix products, arithmetic and copies ran while one was open for 4% -> 0% of each run, Pallas kernels for 0% -> 0%
where the time goes in v1:
time: 160 us; the launch traced here: 159 us
  Pallas kernels  154 us (96%)
  local copies, waits for them, and re-layouts  3.07 us (2%)
    pallas_call x1, Pallas kernels, fused(): pl.pallas_call(functools.partial(kernel, spans), out_shape=(jax.ShapeDtyp...  154 us

profile of v1, /device:TPU:0, one launch (start us, length us, event | category | flops | bytes accessed | tf_op | source)
XLA Modules:
  0.0 159.2 jit_solution(3890577491144261863)
XLA Ops:
  0.6 1.3 convert_element_type.3.query_ref
  1.9 154.2 %gated_state.1 = (bf16[4,8,32,128]{3,2,1,0:T(8,128)(2,1)}, bf16[4,1024]{1,0:T(4,128)(2,1)}) custom-call(bf16[4,128,4096]{2,1,0:T(8,128)(2,1)} %tok_in.1, bf16[1024,1024]{1,0:T(8,128)(2,1)} %wf_in.1, bf16[1024,1024]{1,0:T(8,128)(2,1)} %wv_in.1, f32[4,8,128]{2,1,0:T(8,128)} %bitcast.5, f32[1,1024]{1,0:T(1,128)} %bitcast.6, ...), custom_call_target="tpu_custom_call" | custom-call | tf_op jit(solution)/shard_map/gated_state/pallas_call | solution.py:371
  156.1 1.8 %reshape.15 = bf16[4,8,4096]{2,1,0:T(8,128)(2,1)} reshape(bf16[4,8,32,128]{3,2,1,0:T(8,128)(2,1)} %get-tuple-element.4) | data formatting | bytes 524288 | tf_op jit(solution)/shard_map/reshape | solution.py:420
  157.9 1.3 copy.10

commit v2 on v1

--- a/solution.py
+++ b/solution.py
@@ -195,15 +195,22 @@
 
             lax.fori_loop(0, SUB, one, 0)
 
-    for off in range(1, spans):
-        src = lax.rem(z + off, spans)
-        remote(wf_in.at[:, cols_of(0)], w_buf.at[rows_of(src), cols_of(grp)], w_send.at[off - 1], w_recv.at[src], sp=src).wait_recv()
-        weight_pass(src).start()
-    for off in range(1, spans):
-        src = lax.rem(z + off, spans)
-        remote(shift_in, shift.at[src], s_send.at[off - 1], s_recv.at[src], sp=src).wait_recv()
-    for c in locals_:
-        c.wait()
+    def pass_weights(far):
+        for sign in signs:
+            src = z - far * sign
+
+            @pl.when(fits(src))
+            def _():
+                part = w_buf.at[rows_of(src), cols_of(grp)]
+                remote(wf_in.at[:, cols_of(0)], part, w_send.at[0], w_recv.at[src], sp=z - sign).wait_recv()
+                weight_pass(src).start()
+
+    at_end = jnp.logical_or(z == 0, z == spans - 1)
+
+    def far_of(block, sign):
+        near = z - sign
+        late = jnp.logical_or(near == 0, near == spans - 1)
+        return block + 1 - jnp.where(late, 1, 0)
 
     low = low_ref[:, cols_of(z)]
     head_count = shift_in.shape[1]
@@ -212,33 +219,49 @@
         == z * heads + lax.broadcasted_iota(jnp.int32, (head_count, width), 1) // DK
     ).astype(jnp.float32)
     later_mask = (
-        lax.broadcasted_iota(jnp.int32, (span_len, span_len), 1)
-        > lax.broadcasted_iota(jnp.int32, (span_len, span_len), 0)
-    ).astype(jnp.float32)
+        lax.rem(lax.broadcasted_iota(jnp.int32, (span_len, 3 * span_len), 1), span_len)
+        > lax.broadcasted_iota(jnp.int32, (span_len, 3 * span_len), 0)
+    ).astype(jnp.float32).astype(jnp.bfloat16)
     exact = lax.Precision.HIGHEST
 
-    def compute(src, s):
-        both = jnp.dot(tok[src, s], w_buf[...], preferred_element_type=jnp.float32)
-        gates = (1.0 - low) * jax.nn.sigmoid(-both[:, :width])
-        decay = jnp.log1p(-gates) + lax.dot_general(
-            shift[src, s], pick, (((0,), (0,)), ((), ())), precision=exact, preferred_element_type=jnp.float32
-        )
-        later = jnp.dot(later_mask, decay, precision=exact, preferred_element_type=jnp.float32)
-        totals[src, s] = jnp.broadcast_to(jnp.sum(decay, axis=0, keepdims=True), (8, width))
-        weighted = (gates * jnp.exp(later)).astype(jnp.bfloat16)
-        vals = both[:, width:].astype(jnp.bfloat16)
-        for h in range(heads):
-            lanes = slice(h * DK, (h + 1) * DK)
-            states[src, s, h] = lax.dot_general(
-                vals[:, lanes], weighted[:, lanes], (((0,), (0,)), ((), ())), preferred_element_type=jnp.float32
+    def compute(src, first):
+        rows = tok[src, pl.ds(first, 2)].reshape(2 * span_len, tok.shape[-1])
+        both = jnp.dot(rows, w_buf[...], preferred_element_type=jnp.float32)
+        for i in range(2):
+            s = first + i
+            mine = both[i * span_len:(i + 1) * span_len]
+            gates = (1.0 - low) * jax.nn.sigmoid(-mine[:, :width])
+            decay = jnp.log1p(-gates) + lax.dot_general(
+                shift[src, s], pick, (((0,), (0,)), ((), ())), precision=exact, preferred_element_type=jnp.float32
             )
+            parts, left = [], decay
+            for _ in range(3):
+                parts.append(left.astype(jnp.bfloat16))
+                left = left - parts[-1].astype(jnp.float32)
+            later = jnp.dot(later_mask, jnp.concatenate(parts, axis=0), preferred_element_type=jnp.float32)
+            totals[src, s] = jnp.broadcast_to(jnp.sum(decay, axis=0, keepdims=True), (8, width))
+            weighted = (gates * jnp.exp(later)).astype(jnp.bfloat16)
+            vals = mine[:, width:].astype(jnp.bfloat16)
+            for h in range(heads):
+                lanes = slice(h * DK, (h + 1) * DK)
+                states[src, s, h] = lax.dot_general(
+                    vals[:, lanes], weighted[:, lanes], (((0,), (0,)), ((), ())), preferred_element_type=jnp.float32
+                )
 
     def stage(n, carry):
-        far, u = n // SUB + 1, lax.rem(n, SUB)
+        for far in range(1, spans):
+            due = 0 if far == 1 else jnp.where(at_end, 2 * far - 3, 0)
+
+            @pl.when(n == due)
+            def _():
+                pass_weights(far)
+
+        block, u = n // SUB, lax.rem(n, SUB)
         for direction, sign in enumerate(signs):
+            far = far_of(block, sign)
             src = z - far * sign
 
-            @pl.when(jnp.logical_and(n < steps, fits(src)))
+            @pl.when(jnp.logical_and(jnp.logical_and(n < steps, far > 0), fits(src)))
             def _():
                 z_copy(direction, src, u, z - sign).wait_recv()
 
@@ -250,51 +273,58 @@
                 d_copy(0, src, u).start()
 
         last = jnp.maximum(n - 1, 0)
-        last_far, last_u = last // SUB + 1, lax.rem(last, SUB)
+        last_u = lax.rem(last, SUB)
         for direction, sign in enumerate(signs):
+            last_far = far_of(last // SUB, sign)
             last_src = z - last_far * sign
 
-            @pl.when(jnp.logical_and(jnp.logical_and(n >= 1, n <= steps), fits(last_src)))
+            @pl.when(jnp.logical_and(jnp.logical_and(n >= 1, n <= steps), jnp.logical_and(last_far > 0, fits(last_src))))
             def _():
                 here = piece(last_src, x_tp, last_u)
                 remote(here, here, x_send.at[last_src, last_u], x_recv.at[last_src, last_u], tp=x_tp).wait_recv()
                 d_copy(1, last_src, last_u).start()
 
-        @pl.when(n == 1)
+        @pl.when(n == SUB)
         def _():
             for off in range(1, spans):
                 src = lax.rem(z + off, spans)
                 part = w_buf.at[rows_of(src), cols_of(1 - grp)]
                 remote(part, part, y_send.at[src], y_recv.at[src], grp=1 - grp).wait_recv()
-
-        back = n - 1
-        done_far, slot = back // SUB, lax.rem(back, SUB)
-        who = jnp.where(slot == 0, tp, jnp.where(slot == 1, x_tp, jnp.where(slot == 2, c_tp, xc_tp)))
-
-        def one_side(direction, inner):
-            done_src = z - done_far * (1 - 2 * direction)
-            real = jnp.logical_and(fits(done_src), jnp.logical_or(done_far > 0, direction == 0))
-
-            @pl.when(jnp.logical_and(real, n >= 1))
-            def _():
-                for kind in range(2):
-                    @pl.when(jnp.logical_and(done_far > 0, slot == 2 + kind))
-                    def _():
-                        for v in range(SUB):
-                            here = piece(done_src, c_tp if kind == 0 else xc_tp, v)
-                            remote(here, here, d_send.at[kind, done_src, v], d_recv.at[kind, done_src, v], tp=c_tp).wait_recv()
-
-                compute(done_src, who)
+                remote(shift_in, shift.at[src], s_send.at[off - 1], s_recv.at[src], sp=src).wait_recv()
+            for c in locals_:
+                c.wait()
+
+        kind = u // 2
+        pair = 2 * lax.rem(tp // 2 + kind, 2)
+
+        def one_side(side, inner):
+            done_far = jnp.where(side == 2, 0, far_of(block - 1, 1 - 2 * side))
+            done_src = z - done_far * (1 - 2 * side)
+            real = jnp.logical_or(
+                jnp.logical_and(side == 2, block == 1),
+                jnp.logical_and(jnp.logical_and(side < 2, done_far > 0), fits(done_src)),
+            )
+
+            @pl.when(jnp.logical_and(jnp.logical_and(real, n >= SUB), lax.rem(u, 2) == 1))
+            def _():
+                @pl.when(side < 2)
+                def _():
+                    for v in range(SUB):
+                        here = piece(done_src, c_tp + (xc_tp - c_tp) * kind, v)
+                        remote(here, here, d_send.at[kind, done_src, v], d_recv.at[kind, done_src, v], tp=c_tp).wait_recv()
+
+                compute(done_src, pair)
 
             return inner
 
-        return lax.fori_loop(0, 2, one_side, carry)
-
-    lax.fori_loop(0, spans * SUB + 1, stage, 0)
-
+        return lax.fori_loop(0, 3, one_side, carry)
+
+    lax.fori_loop(0, spans * SUB, stage, 0)
+
+    query_all = query_ref[:, cols_of(z)].astype(jnp.float32)
+    query_all = query_all * jax.nn.sigmoid(query_all)
     for s in range(seqs):
-        query = query_ref[pl.ds(s, 1), cols_of(z)]
-        query = query * jax.nn.sigmoid(query)
+        query = query_all[s:s + 1]
         for h in range(heads):
             lanes = slice(h * DK, (h + 1) * DK)
             suffix = jnp.zeros((1, DK), jnp.float32)
@@ -414,7 +444,7 @@
         w_value,
         decay_shift.transpose(0, 2, 1),
         lower_bound.reshape(1, -1),
-        queries.astype(jnp.float32),
+        queries,
         read_gain.reshape(1, -1),
     )
     return cache.reshape(seqs, head_local, own_rows * DV), read

time: 160 us -> 153 us (0.956)
  Pallas kernels: 154 us -> 148 us
    pallas_call x1, Pallas kernels: 154 us -> 148 us  [fused(): pl.pallas_call(functools.partial(kernel, spans), out_shape=(jax.ShapeDtyp...]
where the time goes in v2:
time: 153 us; the launch traced here: 151 us
  Pallas kernels  148 us (97%)
  local copies, waits for them, and re-layouts  3.07 us (2%)
    pallas_call x1, Pallas kernels, fused(): pl.pallas_call(functools.partial(kernel, spans), out_shape=(jax.ShapeDtyp...  148 us

profile of v2, /device:TPU:0, one launch (start us, length us, event | category | flops | bytes accessed | tf_op | source)
XLA Modules:
  0.0 151.4 jit_solution(1151787425853500505)
XLA Ops:
  0.6 147.7 %gated_state.1 = (bf16[4,8,32,128]{3,2,1,0:T(8,128)(2,1)}, bf16[4,1024]{1,0:T(4,128)(2,1)}) custom-call(bf16[4,128,4096]{2,1,0:T(8,128)(2,1)} %tok_in.1, bf16[1024,1024]{1,0:T(8,128)(2,1)} %wf_in.1, bf16[1024,1024]{1,0:T(8,128)(2,1)} %wv_in.1, f32[4,8,128]{2,1,0:T(8,128)} %bitcast.5, f32[1,1024]{1,0:T(1,128)} %bitcast.6, bf16[4,1024]{1,0:T(4,128)(2,1)} %query_ref.1, ...), custom_call_target="tpu_custom_call" | custom-call | tf_op jit(solution)/shard_map/gated_state/pallas_call | solution.py:401
  148.3 1.8 %reshape.15 = bf16[4,8,4096]{2,1,0:T(8,128)(2,1)} reshape(bf16[4,8,32,128]{3,2,1,0:T(8,128)(2,1)} %get-tuple-element.4) | data formatting | bytes 524288 | tf_op jit(solution)/shard_map/reshape | solution.py:450
  150.1 1.3 copy.10
